TPU v7x, 32 devices: a whole 2x2x4 slice. The times are simulated.
32 devices in a mesh: fs: 8 (over z, y), tp: 4 (over x, core).
Axes of the slice: x: 2, y: 2, z: 4, core: 2. Of those that a mesh axis runs over, the one named last changes fastest.
Arguments:
- tokens: bfloat16 [3072, 2048], P('fs'), may hold values from -6 to 6
- first_norm_scale: float32 [2048], replicated, may hold values from 0.1 to 1.9
- recurrent_branch_matrix: bfloat16 [2048, 1024], P('fs', 'tp'), may hold values from -0.125 to 0.125
- gelu_gate_matrix: bfloat16 [2048, 1024], P('fs', 'tp'), may hold values from -0.125 to 0.125
- filter_taps_weight: bfloat16 [4, 1024], P(None, 'tp'), may hold values from -3 to 3
- recurrence_gate_blocks: bfloat16 [16, 64, 64], P('tp'), may hold values from -0.75 to 0.75
- input_gate_blocks: bfloat16 [16, 64, 64], P('tp'), may hold values from -0.75 to 0.75
- base_decay_logits: float32 [1024], P('tp'), may hold values from 4 to 11
- extra_log_decay: float32 [3072, 1024], P('fs', 'tp'), may hold values from -0.7 to 0
- mixer_output_matrix: bfloat16 [2048, 1024], P('fs', 'tp'), may hold values from -0.5 to 0.5
- second_norm_scale: float32 [2048], replicated, may hold values from 0.1 to 1.9
- mixer_up_matrix: bfloat16 [2048, 4096], P('fs', 'tp'), may hold values from -0.125 to 0.125
- mixer_down_matrix: bfloat16 [2048, 4096], P('fs', 'tp'), may hold values from -0.09375 to 0.09375
Outputs:
- layer_out: bfloat16 [3072, 2048], P(('fs', 'tp'))
All inputs are finite; a program needn't handle non-finite values.
Results may differ from a plain program's by a relative error of at most 0.022.
Values may be sent and summed in bfloat16 or wider, within the bound.
A program may use at most 64 MiB of HBM per device.

v0:
```python
import jax
import jax.numpy as jnp
from jax import lax
from jax.sharding import PartitionSpec as P

epsilon = 1e-06
decay_rate_scale = 8.0


def rms_scaled(sequence_token_rows, scales):
    widened = sequence_token_rows.astype(jnp.float32)
    mean_square = jnp.mean(widened * widened, axis=-1, keepdims=True)
    return (widened * lax.rsqrt(mean_square + epsilon) * scales).astype(jnp.bfloat16)


def linear_combine(earlier, later):
    return (earlier[0] * later[0], later[0] * earlier[1] + later[1])


def causal_taps(branch, filter_taps_weight):
    tap_count = filter_taps_weight.shape[0]
    positions = branch.shape[0]
    padded = jnp.pad(branch.astype(jnp.float32), ((tap_count - 1, 0), (0, 0)))
    running = jnp.zeros(branch.shape, jnp.float32)
    for offset in range(tap_count):
        running = running + padded[offset : offset + positions] * filter_taps_weight[offset].astype(
            jnp.float32
        )
    return running.astype(jnp.bfloat16)


def block_map(convolved, blocks):
    positions, channels = convolved.shape
    grouped = convolved.reshape(positions, blocks.shape[0], blocks.shape[1])
    mapped = jnp.einsum("sgi,gij->sgj", grouped, blocks, preferred_element_type=jnp.float32)
    return jax.nn.sigmoid(mapped.reshape(positions, channels))


def contract_columns(left, right):
    return lax.dot_general(
        left, right, (((1,), (1,)), ((), ())), preferred_element_type=jnp.float32
    )


def local(
    tokens,
    first_norm_scale,
    recurrent_branch_matrix,
    gelu_gate_matrix,
    filter_taps_weight,
    recurrence_gate_blocks,
    input_gate_blocks,
    base_decay_logits,
    extra_log_decay,
    mixer_output_matrix,
    second_norm_scale,
    mixer_up_matrix,
    mixer_down_matrix,
):
    positions = tokens.shape[0]
    own_count = positions // lax.axis_size("tp")
    normed = rms_scaled(tokens, first_norm_scale)
    branch_sum = jnp.dot(
        normed,
        lax.all_gather(recurrent_branch_matrix, "fs", axis=0, tiled=True),
        preferred_element_type=jnp.float32,
    )
    gate_sum = jnp.dot(
        normed,
        lax.all_gather(gelu_gate_matrix, "fs", axis=0, tiled=True),
        preferred_element_type=jnp.float32,
    )
    branch = branch_sum.astype(jnp.bfloat16)
    gate_branch = gate_sum.astype(jnp.bfloat16)
    out_full = lax.all_gather(mixer_output_matrix, "fs", axis=0, tiled=True)
    convolved = causal_taps(branch, filter_taps_weight)
    recurrence_gate_value = block_map(convolved, recurrence_gate_blocks)
    admission = block_map(convolved, input_gate_blocks)
    log_keep_factor = (
        decay_rate_scale * recurrence_gate_value * jax.nn.log_sigmoid(base_decay_logits)
        + extra_log_decay
    )
    retain = jnp.exp(log_keep_factor)
    driven = jnp.sqrt(-jnp.expm1(2.0 * log_keep_factor)) * (
        admission * convolved.astype(jnp.float32)
    )
    memory = lax.associative_scan(linear_combine, (retain, driven), axis=0)[1]
    recurrent = (memory * jax.nn.gelu(gate_branch.astype(jnp.float32))).astype(jnp.bfloat16)
    up_full = lax.all_gather(mixer_up_matrix, "fs", axis=0, tiled=True)
    whole_sum = lax.psum(contract_columns(recurrent, out_full).astype(jnp.bfloat16), "tp").astype(
        jnp.float32
    )
    residual_all = (tokens.astype(jnp.float32) + whole_sum).astype(jnp.bfloat16)
    raised = jnp.dot(
        rms_scaled(residual_all, second_norm_scale), up_full, preferred_element_type=jnp.float32
    )
    hidden = jnp.square(jax.nn.relu(raised)).astype(jnp.bfloat16)
    residual = lax.dynamic_slice_in_dim(
        residual_all, lax.axis_index("tp") * own_count, own_count, 0
    )
    down_full = lax.all_gather(mixer_down_matrix, "fs", axis=0, tiled=True)
    channel_sum = lax.psum_scatter(
        contract_columns(hidden, down_full).astype(jnp.bfloat16),
        "tp",
        scatter_dimension=0,
        tiled=True,
    ).astype(jnp.float32)
    return (residual.astype(jnp.float32) + channel_sum).astype(jnp.bfloat16)


def solution(mesh):
    in_specs = (
        P("fs", None),
        P(),
        P("fs", "tp"),
        P("fs", "tp"),
        P(None, "tp"),
        P("tp", None, None),
        P("tp", None, None),
        P("tp"),
        P("fs", "tp"),
        P("fs", "tp"),
        P(),
        P("fs", "tp"),
        P("fs", "tp"),
    )
    out_specs = P(("fs", "tp"), None)
    return jax.shard_map(local, mesh=mesh, in_specs=in_specs, out_specs=out_specs, check_vma=False)
```

profile of v0, /device:TPU:0, one launch (start us, length us, event | category | flops | bytes accessed | tf_op | source)
XLA Modules:
  0.0 372.9 jit_solution(10167174261476025850)
XLA Ops:
  6.5 0.0 copy-start
  6.5 0.0 all-gather.6.cloned.1.call-start
  6.5 0.7 all-gather.6.cloned.1.call-update
  7.3 0.0 all-gather.10.cloned.1.call-start
  7.3 0.7 all-gather.10.cloned.1.call-update
  8.0 0.0 all-gather.8.cloned.1.call-start
  8.1 0.7 all-gather.8.cloned.1.call-update
  8.7 0.0 all-reduce.19.cloned.1.call-start
  8.8 0.8 slice_convert_fusion.3
  9.6 1.8 fusion.3
  11.4 0.7 fusion.59
  12.1 0.0 copy-start.3
  12.1 40.4 %all-gather.6.cloned.1.call-done = bf16[2048,256]{1,0:T(8,128)(2,1)} async-done(((bf16[256,256]{1,0:T(8,128)(2,1)}), bf16[2048,256]{1,0:T(8,128)(2,1)}) %all-gather.6.cloned.1.call-update) | async-done | bytes 1048592 | tf_op jit(solution)/shard_map/all_gather | solution.py:65
  52.5 2.3 fusion.20
  54.8 0.0 copy-start.2
  54.9 0.2 add_convert_fusion.1
  55.0 0.2 copy.20
  55.2 0.0 copy-done
  55.2 0.3 fusion.18
  55.5 0.2 copy.22
  55.7 0.0 copy-done.3
  55.7 0.3 fusion.15
  56.0 0.2 copy.24
  56.2 0.0 copy-done.2
  56.2 0.5 fusion.49
  56.7 0.1 slice.221
  56.8 0.1 slice.222
  57.0 0.1 slice.220
  57.1 0.1 slice.224
  57.2 0.1 fusion.66
  58.3 0.3 slice.278
  58.6 0.3 slice.219
  59.1 0.0 copy-start.1
  59.1 0.0 copy-start.4
  59.6 0.1 pad.69
  59.7 0.1 fusion.44
  59.7 0.1 pad.68
  59.8 33.8 %all-gather.10.cloned.1.call-done = bf16[2048,256]{1,0:T(8,128)(2,1)} async-done(((bf16[256,256]{1,0:T(8,128)(2,1)}), bf16[2048,256]{1,0:T(8,128)(2,1)}) %all-gather.10.cloned.1.call-update) | async-done | bytes 1048592 | tf_op jit(solution)/shard_map/all_gather | solution.py:75
  93.6 41.2 %all-gather.8.cloned.1.call-done = bf16[2048,256]{1,0:T(8,128)(2,1)} async-done(((bf16[256,256]{1,0:T(8,128)(2,1)}), bf16[2048,256]{1,0:T(8,128)(2,1)}) %all-gather.8.cloned.1.call-update) | async-done | bytes 1048592 | tf_op jit(solution)/shard_map/all_gather | solution.py:70
  134.8 0.0 copy-done.1
  134.8 0.0 copy-done.4
  134.8 4.6 %convolution_convert_fusion.1 = bf16[384,2048]{1,0:T(8,128)(2,1)} fusion(bf16[2048,256]{1,0:T(8,128)(2,1)} %all-gather.10.cloned.1.call-done, bf16[2048,256]{1,0:T(8,128)(2,1)} %all-gather.8.cloned.1.call-done, bf16[384,2048]{1,0:T(8,128)(2,1)S(1)} %copy-done.1, f32[2048]{0:T(1024)S(1)} %copy-done.4, f32[384]{0:T(512)S(1)} %add_rsqrt_fusion.1, ...), kind=kOutput, calls=%fused_computation.13 | convolution fusion | flops 810516480 | bytes 6039040 | tf_op jit(solution)/shard_map/dot_general | solution.py:40
  139.4 0.0 all-reduce.19.cloned.1.call-update
  139.5 0.0 copy-start.5
  139.5 0.0 all-gather.12.cloned.1.call-start
  139.5 0.5 all-gather.12.cloned.1.call-update
  140.1 0.0 all-gather.14.cloned.1.call-start
  140.1 0.5 all-gather.14.cloned.1.call-update
  140.6 0.0 reduce-scatter.2.cloned.1.call-start
  140.7 40.5 %all-reduce.19.cloned.1.call-done = bf16[384,2048]{1,0:T(8,128)(2,1)} async-done(((bf16[384,2048]{1,0:T(8,128)(2,1)}), bf16[384,2048]{1,0:T(8,128)(2,1)}) %all-reduce.19.cloned.1.call-update) | async-done | bytes 1572880 | tf_op jit(solution)/shard_map/psum | solution.py:90
  181.2 2.1 fusion
  183.3 72.7 %all-gather.12.cloned.1.call-done = bf16[2048,1024]{1,0:T(8,128)(2,1)} async-done(((bf16[256,1024]{1,0:T(8,128)(2,1)}), bf16[2048,1024]{1,0:T(8,128)(2,1)}) %all-gather.12.cloned.1.call-update) | async-done | bytes 4194320 | tf_op jit(solution)/shard_map/all_gather | solution.py:89
  256.0 73.3 %all-gather.14.cloned.1.call-done = bf16[2048,1024]{1,0:T(8,128)(2,1)} async-done(((bf16[256,1024]{1,0:T(8,128)(2,1)}), bf16[2048,1024]{1,0:T(8,128)(2,1)}) %all-gather.14.cloned.1.call-update) | async-done | bytes 4194320 | tf_op jit(solution)/shard_map/all_gather | solution.py:101
  329.4 0.0 copy-done.5
  329.4 8.1 %convolution_convert_fusion = bf16[384,2048]{1,0:T(8,128)(2,1)} fusion(bf16[2048,1024]{1,0:T(8,128)(2,1)} %all-gather.14.cloned.1.call-done, bf16[2048,1024]{1,0:T(8,128)(2,1)} %all-gather.12.cloned.1.call-done, bf16[384,2048]{1,0:T(8,128)(2,1)S(1)} %get-tuple-element.6, f32[2048]{0:T(1024)S(1)} %copy-done.5, f32[384]{0:T(512)S(1)} %add_rsqrt_fusion), kind=kOutput, calls=%fused_computation.12 | convolution fusion | flops 3226337280 | bytes 11544064 | tf_op jit(solution)/shard_map/dot_general | solution.py:40
  337.5 0.0 reduce-scatter.2.cloned.1.call-update
  337.6 26.7 %reduce-scatter.2.cloned.1.call-done = bf16[96,2048]{1,0:T(8,128)(2,1)} async-done(((bf16[384,2048]{1,0:T(8,128)(2,1)}), bf16[96,2048]{1,0:T(8,128)(2,1)}) %reduce-scatter.2.cloned.1.call-update) | async-done | bytes 393232 | tf_op jit(solution)/shard_map/reduce_scatter | solution.py:102
  364.2 1.8 add_convert_fusion
  (86 shorter events, 1.3 us)
Async XLA Ops:
  6.5 48.7 %copy-start = (bf16[4,64,64]{2,1,0:T(8,128)(2,1)S(1)}, bf16[4,64,64]{2,1,0:T(8,128)(2,1)}, u32[]{:S(2)}) copy-start(bf16[4,64,64]{2,1,0:T(8,128)(2,1)} %param.18) | copy-start | bytes 98308
  6.5 46.0 %all-gather.6.cloned.1.call-start = ((), (), s32[]{:S(2)}) async-start(), calls=%async_computation.1 | async-start | bytes 1179648 | tf_op jit(solution)/shard_map/all_gather | solution.py:65
  7.3 86.4 %all-gather.10.cloned.1.call-start = ((), (), s32[]{:S(2)}) async-start(), calls=%async_computation.3 | async-start | bytes 1179648 | tf_op jit(solution)/shard_map/all_gather | solution.py:75
  8.0 126.8 %all-gather.8.cloned.1.call-start = ((), (), s32[]{:S(2)}) async-start(), calls=%async_computation.2 | async-start | bytes 1179648 | tf_op jit(solution)/shard_map/all_gather | solution.py:70
  8.7 172.4 %all-reduce.19.cloned.1.call-start = ((), (), s32[]{:S(2)}) async-start(), calls=%async_computation.4 | async-start | bytes 3145728 | tf_op jit(solution)/shard_map/psum | solution.py:90
  12.1 43.6 %copy-start.3 = (bf16[4,64,64]{2,1,0:T(8,128)(2,1)S(1)}, bf16[4,64,64]{2,1,0:T(8,128)(2,1)}, u32[]{:S(2)}) copy-start(bf16[4,64,64]{2,1,0:T(8,128)(2,1)} %param.19) | copy-start | bytes 98308
  54.8 1.4 copy-start.2
  59.1 75.7 %copy-start.1 = (bf16[384,2048]{1,0:T(8,128)(2,1)S(1)}, bf16[384,2048]{1,0:T(8,128)(2,1)}, u32[]{:S(2)}) copy-start(bf16[384,2048]{1,0:T(8,128)(2,1)} %param.13) | copy-start | bytes 4718596
  59.1 75.7 %copy-start.4 = (f32[2048]{0:T(1024)S(1)}, f32[2048]{0:T(1024)}, u32[]{:S(2)}) copy-start(f32[2048]{0:T(1024)} %param.14) | copy-start | bytes 24580
  139.5 189.9 %copy-start.5 = (f32[2048]{0:T(1024)S(1)}, f32[2048]{0:T(1024)}, u32[]{:S(2)}) copy-start(f32[2048]{0:T(1024)} %param.23) | copy-start | bytes 24580
  139.5 116.6 %all-gather.12.cloned.1.call-start = ((), (), s32[]{:S(2)}) async-start(), calls=%async_computation.5 | async-start | bytes 4718592 | tf_op jit(solution)/shard_map/all_gather | solution.py:89
  140.1 189.3 %all-gather.14.cloned.1.call-start = ((), (), s32[]{:S(2)}) async-start(), calls=%async_computation.6 | async-start | bytes 4718592 | tf_op jit(solution)/shard_map/all_gather | solution.py:101
  140.6 223.6 %reduce-scatter.2.cloned.1.call-start = ((), (), s32[]{:S(2)}) async-start(), calls=%async_computation.7 | async-start | bytes 1966080 | tf_op jit(solution)/shard_map/reduce_scatter | solution.py:102
Sparse Core Ops, SparseCore 0:
  9.5 42.9 all-gather.5
  54.6 38.9 all-gather.9
  95.8 38.9 all-gather.7
  139.6 41.5 all-reduce.18
  183.2 72.8 all-gather.11
  258.0 71.3 all-gather.13
  337.7 26.5 reduce-scatter.1
where the time goes:
time: 373 us
  waiting for transfers between devices  332 us (89%)
  matrix products  15.7 us (4%)
  between operations  14.1 us (4%)
  other arithmetic  8.42 us (2%)
    all_gather x1, waiting for transfers between devices, local(): down_full = lax.all_gather(mixer_down_matrix, 'fs', axis=0, tiled=True)  73.3 us
    all_gather x1, waiting for transfers between devices, local(): up_full = lax.all_gather(mixer_up_matrix, 'fs', axis=0, tiled=True)  72.7 us
    all_gather x1, waiting for transfers between devices, local(): lax.all_gather(gelu_gate_matrix, 'fs', axis=0, tiled=True)  41.2 us
    psum x1, waiting for transfers between devices, local(): lax.psum(contract_columns(recurrent, out_full).astype(jnp.bfloat16), 'tp')  40.5 us
    all_gather x1, waiting for transfers between devices, local(): lax.all_gather(recurrent_branch_matrix, 'fs', axis=0, tiled=True)  40.4 us
    all_gather x1, waiting for transfers between devices, local(): out_full = lax.all_gather(mixer_output_matrix, 'fs', axis=0, tiled=True)  33.8 us
    reduce_scatter x1, waiting for transfers between devices, local(): lax.psum_scatter(contract_columns(hidden, down_full).astype(jnp.bfloat16)...  26.7 us
    dot_general x2, matrix products, contract_columns(): lax.dot_general(left, right, (((1,), (1,)), ((), ())), preferred_element_...  12.8 us
  transfers between devices with their start and end apart: 7, of which 7 were waited for; matrix products, arithmetic and copies ran while one was open for 3% of the time, Pallas kernels for 0%

commit v1 on v0

--- a/solution.py
+++ b/solution.py
@@ -72,7 +72,12 @@
     )
     branch = branch_sum.astype(jnp.bfloat16)
     gate_branch = gate_sum.astype(jnp.bfloat16)
-    out_full = lax.all_gather(mixer_output_matrix, "fs", axis=0, tiled=True)
+    ring = [mixer_output_matrix]
+    for hop in range(7):
+        ring.append(lax.ppermute(ring[-1], "fs", [(dev, (dev + 1) % 8) for dev in range(8)]))
+    out_full = jnp.roll(
+        jnp.concatenate(ring[::-1], axis=0), (lax.axis_index("fs") + 1) * ring[0].shape[0], axis=0
+    )
     convolved = causal_taps(branch, filter_taps_weight)
     recurrence_gate_value = block_map(convolved, recurrence_gate_blocks)
     admission = block_map(convolved, input_gate_blocks)

time: 373 us -> 335 us (0.90)
  waiting for transfers between devices: 332 us -> 277 us
  local copies, waits for them, and re-layouts: 2.7 us -> 14.7 us
    ppermute x0 -> x7, waiting for transfers between devices: none -> 52.1 us  [local(): lax.ppermute(ring[-1], 'fs', [(dev, (dev + 1) % 8) for dev in range(8)])]
    all_gather x1, waiting for transfers between devices: 40.4 us -> 0.01 us  [local(): lax.all_gather(recurrent_branch_matrix, 'fs', axis=0, tiled=True)]
    all_gather x1 -> x0, waiting for transfers between devices: 33.8 us -> none  [local(): out_full = lax.all_gather(mixer_output_matrix, 'fs', axis=0, tiled=True)]
    all_gather x1, waiting for transfers between devices: 41.2 us -> 9.51 us  [local(): lax.all_gather(gelu_gate_matrix, 'fs', axis=0, tiled=True)]
    unnamed x12 -> x27, local copies, waits for them, and re-layouts: 0.03 us -> 9.96 us
  transfers between devices with their start and end apart: 7 -> 13, of which waited for: 7 -> 12; matrix products, arithmetic and copies ran while one was open for 3% -> 8% of each run, Pallas kernels for 0% -> 0%
where the time goes in v1:
time: 335 us; the launch traced here: 334 us
  waiting for transfers between devices  277 us (83%)
  matrix products  15.2 us (5%)
  local copies, waits for them, and re-layouts  14.7 us (4%)
  between operations  14.1 us (4%)
  other arithmetic  10.4 us (3%)
    all_gather x1, waiting for transfers between devices, local(): up_full = lax.all_gather(mixer_up_matrix, 'fs', axis=0, tiled=True)  73.3 us
    all_gather x1, waiting for transfers between devices, local(): down_full = lax.all_gather(mixer_down_matrix, 'fs', axis=0, tiled=True)  72.7 us
    ppermute x7, waiting for transfers between devices, local(): lax.ppermute(ring[-1], 'fs', [(dev, (dev + 1) % 8) for dev in range(8)])  52.1 us
    psum x1, waiting for transfers between devices, local(): lax.psum(contract_columns(recurrent, out_full).astype(jnp.bfloat16), 'tp')  40.5 us
    reduce_scatter x1, waiting for transfers between devices, local(): lax.psum_scatter(contract_columns(hidden, down_full).astype(jnp.bfloat16)...  26.7 us
    dot_general x2, matrix products, contract_columns(): lax.dot_general(left, right, (((1,), (1,)), ((), ())), preferred_element_...  12.7 us
    unnamed x27, local copies, waits for them, and re-layouts  9.96 us
    all_gather x1, waiting for transfers between devices, local(): lax.all_gather(gelu_gate_matrix, 'fs', axis=0, tiled=True)  9.51 us
  transfers between devices with their start and end apart: 13, of which 12 were waited for; matrix products, arithmetic and copies ran while one was open for 8% of the time, Pallas kernels for 0%

profile of v1, /device:TPU:0, one launch (start us, length us, event | category | flops | bytes accessed | tf_op | source)
XLA Modules:
  0.0 334.3 jit_solution(12055099338860707008)
XLA Ops:
  6.5 0.7 all-gather.5.cloned.1.call-update
  7.3 0.0 all-gather.7.cloned.1.call-start
  7.3 3.0 collective-permute-start
  10.4 6.7 %collective-permute-done = bf16[256,256]{1,0:T(8,128)(2,1)S(1)} collective-permute-done((bf16[256,256]{1,0:T(8,128)(2,1)}, bf16[256,256]{1,0:T(8,128)(2,1)S(1)}, u32[]{:S(2)}, u32[]{:S(2)}) %collective-permute-start) | collective-permute-done | bytes 131104 | tf_op jit(solution)/shard_map/ppermute | solution.py:77
  17.1 7.8 %collective-permute-done.1 = bf16[256,256]{1,0:T(8,128)(2,1)S(1)} collective-permute-done((bf16[256,256]{1,0:T(8,128)(2,1)S(1)}, bf16[256,256]{1,0:T(8,128)(2,1)S(1)}, u32[]{:S(2)}, u32[]{:S(2)}) %collective-permute-start.1) | collective-permute-done | bytes 131104 | tf_op jit(solution)/shard_map/ppermute | solution.py:77
  24.9 0.0 all-gather.7.cloned.1.call-update
  24.9 0.0 all-reduce.19.cloned.1.call-start
  25.0 8.2 %collective-permute-done.2 = bf16[256,256]{1,0:T(8,128)(2,1)S(1)} collective-permute-done((bf16[256,256]{1,0:T(8,128)(2,1)S(1)}, bf16[256,256]{1,0:T(8,128)(2,1)S(1)}, u32[]{:S(2)}, u32[]{:S(2)}) %collective-permute-start.2) | collective-permute-done | bytes 131104 | tf_op jit(solution)/shard_map/ppermute | solution.py:77
  33.1 0.8 slice_convert_fusion.3
  34.0 6.9 %collective-permute-done.3 = bf16[256,256]{1,0:T(8,128)(2,1)S(1)} collective-permute-done((bf16[256,256]{1,0:T(8,128)(2,1)S(1)}, bf16[256,256]{1,0:T(8,128)(2,1)S(1)}, u32[]{:S(2)}, u32[]{:S(2)}) %collective-permute-start.3) | collective-permute-done | bytes 131104 | tf_op jit(solution)/shard_map/ppermute | solution.py:77
  40.9 1.8 fusion.3
  42.7 7.9 %collective-permute-done.4 = bf16[256,256]{1,0:T(8,128)(2,1)S(1)} collective-permute-done((bf16[256,256]{1,0:T(8,128)(2,1)S(1)}, bf16[256,256]{1,0:T(8,128)(2,1)S(1)}, u32[]{:S(2)}, u32[]{:S(2)}) %collective-permute-start.4) | collective-permute-done | bytes 131104 | tf_op jit(solution)/shard_map/ppermute | solution.py:77
  50.6 7.7 %collective-permute-done.5 = bf16[256,256]{1,0:T(8,128)(2,1)S(1)} collective-permute-done((bf16[256,256]{1,0:T(8,128)(2,1)S(1)}, bf16[256,256]{1,0:T(8,128)(2,1)S(1)}, u32[]{:S(2)}, u32[]{:S(2)}) %collective-permute-start.5) | collective-permute-done | bytes 131104 | tf_op jit(solution)/shard_map/ppermute | solution.py:77
  58.2 0.7 fusion.60
  58.9 7.0 %collective-permute-done.6 = bf16[256,256]{1,0:T(8,128)(2,1)S(1)} collective-permute-done((bf16[256,256]{1,0:T(8,128)(2,1)S(1)}, bf16[256,256]{1,0:T(8,128)(2,1)S(1)}, u32[]{:S(2)}, u32[]{:S(2)}) %collective-permute-start.6) | collective-permute-done | bytes 131104 | tf_op jit(solution)/shard_map/ppermute | solution.py:77
  65.9 0.7 constant_dynamic-update-slice_fusion.15
  66.6 0.7 constant_dynamic-update-slice_fusion.14
  67.2 0.7 constant_dynamic-update-slice_fusion.13
  67.9 0.7 constant_dynamic-update-slice_fusion.12
  68.5 0.7 constant_dynamic-update-slice_fusion.11
  69.2 0.7 constant_dynamic-update-slice_fusion.10
  69.9 0.7 constant_dynamic-update-slice_fusion.9
  70.5 0.7 constant_dynamic-update-slice_fusion.8
  71.2 0.7 constant_dynamic-update-slice_fusion.7
  71.9 0.7 constant_dynamic-update-slice_fusion.6
  72.5 0.7 constant_dynamic-update-slice_fusion.5
  73.2 0.7 constant_dynamic-update-slice_fusion.4
  73.8 0.7 constant_dynamic-update-slice_fusion.3
  74.5 0.7 constant_dynamic-update-slice_fusion.2
  75.2 0.7 constant_dynamic-update-slice_fusion.1
  75.8 0.7 constant_dynamic-update-slice_fusion
  76.5 1.8 fusion.20
  78.4 0.2 add_convert_fusion.1
  78.6 0.2 copy.20
  78.7 0.3 fusion.18
  79.1 0.2 copy.22
  79.2 0.3 fusion.15
  79.6 0.9 copy.24
  80.5 1.6 fusion.50
  82.1 0.1 slice.221
  82.2 0.1 slice.222
  82.3 0.1 slice.220
  82.5 0.7 slice.224
  83.2 1.0 fusion.68
  85.2 0.3 slice.278
  85.5 0.3 slice.219
  86.5 0.1 pad.69
  86.5 0.1 fusion.45
  86.6 0.1 pad.68
  86.7 9.5 %all-gather.7.cloned.1.call-done = bf16[2048,256]{1,0:T(8,128)(2,1)} async-done(((bf16[256,256]{1,0:T(8,128)(2,1)}), bf16[2048,256]{1,0:T(8,128)(2,1)}) %all-gather.7.cloned.1.call-update) | async-done | bytes 1048592 | tf_op jit(solution)/shard_map/all_gather | solution.py:70
  96.2 4.6 %convolution_convert_fusion.1 = bf16[384,2048]{1,0:T(8,128)(2,1)} fusion(bf16[4096,256]{1,0:T(8,128)(2,1)} %constant_dynamic-update-slice_fusion, s32[]{:T(128)S(6)} %select_n.23, bf16[2048,256]{1,0:T(8,128)(2,1)} %all-gather.7.cloned.1.call-done, bf16[384,2048]{1,0:T(8,128)(2,1)S(1)} %copy-done.1, f32[2048]{0:T(1024)S(1)} %copy-done.4, ...), kind=kOutput, calls=%fused_computation.13 | convolution fusion | flops 810516480 | bytes 6039044 | tf_op jit(solution)/shard_map/dot_general | solution.py:40
  100.8 0.0 all-reduce.19.cloned.1.call-update
  100.8 0.0 all-gather.11.cloned.1.call-start
  100.9 0.5 all-gather.11.cloned.1.call-update
  101.4 0.0 all-gather.9.cloned.1.call-start
  101.4 0.5 all-gather.9.cloned.1.call-update
  102.0 0.0 reduce-scatter.2.cloned.1.call-start
  102.0 40.5 %all-reduce.19.cloned.1.call-done = bf16[384,2048]{1,0:T(8,128)(2,1)} async-done(((bf16[384,2048]{1,0:T(8,128)(2,1)}), bf16[384,2048]{1,0:T(8,128)(2,1)}) %all-reduce.19.cloned.1.call-update) | async-done | bytes 1572880 | tf_op jit(solution)/shard_map/psum | solution.py:95
  142.5 2.1 fusion
  144.7 72.7 %all-gather.11.cloned.1.call-done = bf16[2048,1024]{1,0:T(8,128)(2,1)} async-done(((bf16[256,1024]{1,0:T(8,128)(2,1)}), bf16[2048,1024]{1,0:T(8,128)(2,1)}) %all-gather.11.cloned.1.call-update) | async-done | bytes 4194320 | tf_op jit(solution)/shard_map/all_gather | solution.py:106
  217.4 73.3 %all-gather.9.cloned.1.call-done = bf16[2048,1024]{1,0:T(8,128)(2,1)} async-done(((bf16[256,1024]{1,0:T(8,128)(2,1)}), bf16[2048,1024]{1,0:T(8,128)(2,1)}) %all-gather.9.cloned.1.call-update) | async-done | bytes 4194320 | tf_op jit(solution)/shard_map/all_gather | solution.py:94
  290.8 8.1 %convolution_convert_fusion = bf16[384,2048]{1,0:T(8,128)(2,1)} fusion(bf16[2048,1024]{1,0:T(8,128)(2,1)} %all-gather.11.cloned.1.call-done, bf16[2048,1024]{1,0:T(8,128)(2,1)} %all-gather.9.cloned.1.call-done, bf16[384,2048]{1,0:T(8,128)(2,1)S(1)} %get-tuple-element.6, f32[2048]{0:T(1024)S(1)} %copy-done.5, f32[384]{0:T(512)S(1)} %add_rsqrt_fusion), kind=kOutput, calls=%fused_computation.12 | convolution fusion | flops 3226337280 | bytes 11544064 | tf_op jit(solution)/shard_map/dot_general | solution.py:40
  298.9 26.7 %reduce-scatter.2.cloned.1.call-done = bf16[96,2048]{1,0:T(8,128)(2,1)} async-done(((bf16[384,2048]{1,0:T(8,128)(2,1)}), bf16[96,2048]{1,0:T(8,128)(2,1)}) %reduce-scatter.2.cloned.1.call-update) | async-done | bytes 393232 | tf_op jit(solution)/shard_map/reduce_scatter | solution.py:107
  325.6 1.8 add_convert_fusion
  (107 shorter events, 1.4 us)
Async XLA Ops:
  6.5 72.2 %copy-start = (bf16[4,64,64]{2,1,0:T(8,128)(2,1)S(1)}, bf16[4,64,64]{2,1,0:T(8,128)(2,1)}, u32[]{:S(2)}) copy-start(bf16[4,64,64]{2,1,0:T(8,128)(2,1)} %param.18) | copy-start | bytes 98308
  6.5 64.0 %copy-start.2 = (bf16[256,256]{1,0:T(8,128)(2,1)S(1)}, bf16[256,256]{1,0:T(8,128)(2,1)}, u32[]{:S(2)}) copy-start(bf16[256,256]{1,0:T(8,128)(2,1)} %param.22) | copy-start | bytes 393220
  6.5 70.0 %all-gather.5.cloned.1.call-start = ((), (), s32[]{:S(2)}) async-start(), calls=%async_computation.1 | async-start | bytes 1179648 | tf_op jit(solution)/shard_map/all_gather | solution.py:65
  7.3 88.9 %all-gather.7.cloned.1.call-start = ((), (), s32[]{:S(2)}) async-start(), calls=%async_computation.2 | async-start | bytes 1179648 | tf_op jit(solution)/shard_map/all_gather | solution.py:70
  7.3 9.8 %collective-permute-start = (bf16[256,256]{1,0:T(8,128)(2,1)}, bf16[256,256]{1,0:T(8,128)(2,1)S(1)}, u32[]{:S(2)}, u32[]{:S(2)}) collective-permute-start(bf16[256,256]{1,0:T(8,128)(2,1)} %param.22), channel_id=1, source_target_pairs={{0,4},{4,8},{8,12},{12,16},{16,20},{20,24},{24,28},{28,0},{1,5},{5... | collective-permute-start | bytes 393224 | tf_op jit(solution)/shard_map/ppermute | solution.py:77
  17.1 7.8 %collective-permute-start.1 = (bf16[256,256]{1,0:T(8,128)(2,1)S(1)}, bf16[256,256]{1,0:T(8,128)(2,1)S(1)}, u32[]{:S(2)}, u32[]{:S(2)}) collective-permute-start(bf16[256,256]{1,0:T(8,128)(2,1)S(1)} %collective-permute-done), channel_id=1, source_target_pairs={{0,4},{4,8},{8,12},{12,16},{16,20},{20,24},{24,28},{28,0},{1,5},{5... | collective-permute-start | bytes 393224 | tf_op jit(solution)/shard_map/ppermute | solution.py:77
  24.9 8.3 %collective-permute-start.2 = (bf16[256,256]{1,0:T(8,128)(2,1)S(1)}, bf16[256,256]{1,0:T(8,128)(2,1)S(1)}, u32[]{:S(2)}, u32[]{:S(2)}) collective-permute-start(bf16[256,256]{1,0:T(8,128)(2,1)S(1)} %collective-permute-done.1), channel_id=1, source_target_pairs={{0,4},{4,8},{8,12},{12,16},{16,20},{20,24},{24,28},{28,0},{1,5},{5... | collective-permute-start | bytes 393224 | tf_op jit(solution)/shard_map/ppermute | solution.py:77
  24.9 117.7 %all-reduce.19.cloned.1.call-start = ((), (), s32[]{:S(2)}) async-start(), calls=%async_computation.3 | async-start | bytes 3145728 | tf_op jit(solution)/shard_map/psum | solution.py:95
  33.1 7.8 %collective-permute-start.3 = (bf16[256,256]{1,0:T(8,128)(2,1)S(1)}, bf16[256,256]{1,0:T(8,128)(2,1)S(1)}, u32[]{:S(2)}, u32[]{:S(2)}) collective-permute-start(bf16[256,256]{1,0:T(8,128)(2,1)S(1)} %collective-permute-done.2), channel_id=1, source_target_pairs={{0,4},{4,8},{8,12},{12,16},{16,20},{20,24},{24,28},{28,0},{1,5},{5... | collective-permute-start | bytes 393224 | tf_op jit(solution)/shard_map/ppermute | solution.py:77
  40.9 9.7 %collective-permute-start.4 = (bf16[256,256]{1,0:T(8,128)(2,1)S(1)}, bf16[256,256]{1,0:T(8,128)(2,1)S(1)}, u32[]{:S(2)}, u32[]{:S(2)}) collective-permute-start(bf16[256,256]{1,0:T(8,128)(2,1)S(1)} %collective-permute-done.3), channel_id=1, source_target_pairs={{0,4},{4,8},{8,12},{12,16},{16,20},{20,24},{24,28},{28,0},{1,5},{5... | collective-permute-start | bytes 393224 | tf_op jit(solution)/shard_map/ppermute | solution.py:77
  50.6 7.7 %collective-permute-start.5 = (bf16[256,256]{1,0:T(8,128)(2,1)S(1)}, bf16[256,256]{1,0:T(8,128)(2,1)S(1)}, u32[]{:S(2)}, u32[]{:S(2)}) collective-permute-start(bf16[256,256]{1,0:T(8,128)(2,1)S(1)} %collective-permute-done.4), channel_id=1, source_target_pairs={{0,4},{4,8},{8,12},{12,16},{16,20},{20,24},{24,28},{28,0},{1,5},{5... | collective-permute-start | bytes 393224 | tf_op jit(solution)/shard_map/ppermute | solution.py:77
  58.2 7.7 %collective-permute-start.6 = (bf16[256,256]{1,0:T(8,128)(2,1)S(1)}, bf16[256,256]{1,0:T(8,128)(2,1)S(1)}, u32[]{:S(2)}, u32[]{:S(2)}) collective-permute-start(bf16[256,256]{1,0:T(8,128)(2,1)S(1)} %collective-permute-done.5), channel_id=1, source_target_pairs={{0,4},{4,8},{8,12},{12,16},{16,20},{20,24},{24,28},{28,0},{1,5},{5... | collective-permute-start | bytes 393224 | tf_op jit(solution)/shard_map/ppermute | solution.py:77
  58.9 17.6 %copy-start.1 = (bf16[384,2048]{1,0:T(8,128)(2,1)S(1)}, bf16[384,2048]{1,0:T(8,128)(2,1)}, u32[]{:S(2)}) copy-start(bf16[384,2048]{1,0:T(8,128)(2,1)} %param.13) | copy-start | bytes 4718596
  58.9 17.6 %copy-start.4 = (f32[2048]{0:T(1024)S(1)}, f32[2048]{0:T(1024)}, u32[]{:S(2)}) copy-start(f32[2048]{0:T(1024)} %param.14) | copy-start | bytes 24580
  78.4 0.9 copy-start.3
  100.8 116.6 %all-gather.11.cloned.1.call-start = ((), (), s32[]{:S(2)}) async-start(), calls=%async_computation.5 | async-start | bytes 4718592 | tf_op jit(solution)/shard_map/all_gather | solution.py:106
  101.4 189.3 %all-gather.9.cloned.1.call-start = ((), (), s32[]{:S(2)}) async-start(), calls=%async_computation.4 | async-start | bytes 4718592 | tf_op jit(solution)/shard_map/all_gather | solution.py:94
  102.0 188.8 %copy-start.5 = (f32[2048]{0:T(1024)S(1)}, f32[2048]{0:T(1024)}, u32[]{:S(2)}) copy-start(f32[2048]{0:T(1024)} %param.23) | copy-start | bytes 24580
  102.0 223.6 %reduce-scatter.2.cloned.1.call-start = ((), (), s32[]{:S(2)}) async-start(), calls=%async_computation.6 | async-start | bytes 1966080 | tf_op jit(solution)/shard_map/reduce_scatter | solution.py:107
Sparse Core Ops, SparseCore 0:
  9.5 45.0 all-gather.4
  56.7 39.4 all-gather.6
  100.9 41.5 all-reduce.18
  144.5 72.8 all-gather.10
  219.4 71.3 all-gather.8
  299.0 26.5 reduce-scatter.1
